TPU v7x, 32 devices: a whole 2x2x4 slice. The times are simulated.
32 devices in a mesh: rep: 2 (over x), fs: 8 (over z, y), tp: 2 (over core).
Axes of the slice: x: 2, y: 2, z: 4, core: 2. Of those that a mesh axis runs over, the one named last changes fastest.
Arguments:
- x_late: bfloat16 [2048, 2048], P(('rep', 'fs')), parts along dimension 0, may hold values from -6 to 6
- x_early: bfloat16 [2048, 2048], P(('rep', 'fs')), parts along dimension 0, may hold values from -6 to 6
- cotangent: bfloat16 [2048, 2048], P(('rep', 'fs')), parts along dimension 0, may hold values from -6 to 6
- pre_gain: float32 [2048], replicated, may hold values from 0.1 to 1.9
- post_gain: float32 [2048], replicated, may hold values from 0.1 to 1.9
- gate_weight: bfloat16 [2048, 3072], P('fs', 'tp'), may hold values from -0.125 to 0.125
- up_weight: bfloat16 [2048, 3072], P('fs', 'tp'), may hold values from -0.125 to 0.125
- down_weight: bfloat16 [2048, 3072], P('fs', 'tp'), may hold values from -0.109375 to 0.109375
- down_grad_sum: float32 [4096, 3072], P(('rep', 'fs'), 'tp'), parts along dimension 0, may hold values from -6 to 6
Outputs:
- y_late: bfloat16 [2048, 2048], P(('rep', 'fs')), parts along dimension 0
- dx_early: bfloat16 [2048, 2048], P(('rep', 'fs')), parts along dimension 0
- down_grad_out: float32 [4096, 3072], P(('rep', 'fs'), 'tp'), parts along dimension 0
There are 2 independent parts, one for each index of `rep`. A program takes and returns all parts, laid end to end along the dimension named above; an argument that names none is the same for every part. Nothing has to cross between parts.
All inputs are finite; a program needn't handle non-finite values.
Results may differ from a plain program's by a relative error of at most 0.023.
Values may be sent and summed in bfloat16 or wider, within the bound.
A program may use at most 64 MiB of HBM per device.

v0:
```python
import functools
import itertools

import jax
import jax.numpy as jnp
from jax import lax
from jax.experimental import pallas as pl
from jax.experimental.pallas import tpu as pltpu
from jax.sharding import PartitionSpec as P

eps = 1e-06
F32, BF16 = jnp.float32, jnp.bfloat16
VMEM = pl.BlockSpec(memory_space=pltpu.VMEM)
DMA = pltpu.SemaphoreType.DMA


class Grid:
    def __init__(self, sizes):
        self.R, self.fs, self.tp = sizes
        self.fy = 2
        self.fz = self.fs // self.fy
        self.G = self.R * self.fy
        self.offsets = list(itertools.product(range(self.R), range(self.fy)))[1:]
        self.r, f, self.k = (lax.axis_index(n) for n in ("rep", "fs", "tp"))
        self.z, self.y = lax.div(f, self.fy), lax.rem(f, self.fy)
        self.g = self.r * self.fy + self.y

    def moved(self, o, sign=1):
        dr, dy = self.offsets[o]
        r = lax.rem(self.r + self.R + sign * dr, self.R)
        y = lax.rem(self.y + self.fy + sign * dy, self.fy)
        return r, y

    def index(self, o, sign=1):
        r, y = self.moved(o, sign)
        return r * self.fy + y

    def peer(self, o):
        r, y = self.moved(o)
        return {"rep": r, "fs": self.z * self.fy + y, "tp": self.k}

    def sibling_index(self, j):
        return lax.rem(self.k + j, self.tp)

    def sibling(self, j):
        return {"rep": self.r, "fs": self.z * self.fy + self.y, "tp": self.sibling_index(j)}

    def along(self, step):
        return lax.rem(self.z + self.fz + step, self.fz)

    def level(self, step):
        return {"rep": self.r, "fs": self.along(step) * self.fy + self.y, "tp": self.k}

    def barrier(self, group=False, pair=False, ring=False, levels=False):
        sem = pltpu.get_barrier_semaphore()
        targets = []
        if group:
            targets += [self.peer(o) for o in range(len(self.offsets))]
        if pair:
            targets += [self.sibling(j) for j in range(1, self.tp)]
        if levels:
            targets += [self.level(s) for s in range(1, self.fz)]
        elif ring:
            targets += [self.level(1), self.level(-1)]
        for t in targets:
            pl.semaphore_signal(sem, inc=1, device_id=t, device_id_type=pl.DeviceIdType.MESH)
        pl.semaphore_wait(sem, len(targets))


class Copies:
    def __init__(self, sems):
        self.sems, self.used = sems, 0

    def push(self, src, dst, to):
        copy = pltpu.make_async_remote_copy(
            src_ref=src, dst_ref=dst, send_sem=self.sems.at[0, self.used], recv_sem=self.sems.at[1, self.used],
            device_id=to, device_id_type=pl.DeviceIdType.MESH,
        )
        self.used += 1
        copy.start()
        return copy


class Ring:
    def __init__(self, m, cp, first, slot, chunks):
        self.m, self.cp, self.first, self.slot = m, cp, first, slot
        self.order = {0: chunks, 1: chunks[len(chunks) // 2:] + chunks[:len(chunks) // 2]}
        self.fronts = {0: set(chunks[: len(chunks) // 2]), 1: set(chunks[len(chunks) // 2:])}
        self.half = m.fz // 2
        self.sent, self.arrived = {}, set()

    def send(self, d, s, c):
        sign = 1 if d == 0 else -1
        block = self.m.along(-sign * (s - 1))
        src = self.first(c) if s == 1 else self.slot(block, c)
        self.sent[d, s, c] = self.cp.push(src, self.slot(block, c), self.m.level(sign))

    def arrive(self, d, s, c):
        if (d, s, c) not in self.sent or (d, s, c) in self.arrived:
            return
        self.sent[d, s, c].wait_recv()
        self.arrived.add((d, s, c))
        if s + 1 < self.half or (s + 1 == self.half and c in self.fronts[d]):
            self.send(d, s + 1, c)

    def step(self, s, ds=(0, 1)):
        for i in range(len(self.order[0])):
            for d in ds:
                self.arrive(d, s, self.order[d][i])

    def finish(self):
        for copy in self.sent.values():
            copy.wait_send()


def stages(m):
    half = m.fz // 2
    out = [(0, 0, ())]
    for s in range(1, half):
        out += [(-s, s, (0,)), (s, s, (1,))]
    return out + [(half, half, (0, 1))]


class Scatter:
    def __init__(self, m, cp, p, rx, tx, rg, acc, place):
        self.m, self.cp, self.p, self.rx, self.tx, self.rg, self.acc = m, cp, p, rx, tx, rg, acc
        self.place = place
        self.pair, self.far = {}, {}

    def start(self, t):
        m = self.m
        for j in range(1, m.tp):
            src = self.p.at[t, :, :, m.sibling_index(j)]
            self.pair[t, j] = self.cp.push(src, self.rx.at[j - 1, t], m.sibling(j))

    def middle(self, t):
        m, n = self.m, len(self.m.offsets)
        for j in range(1, m.tp):
            self.pair[t, j].wait_recv()

        def total(block):
            value = self.p[t, :, block, m.k].astype(F32)
            for j in range(1, m.tp):
                value = value + self.rx[j - 1, t, :, block].astype(F32)
            return value

        for o in range(n):
            self.tx[t, o] = total(m.index(o)).astype(BF16)
            self.far[t, o] = self.cp.push(self.tx.at[t, o], self.rg.at[t, o], m.peer(o))
        self.acc[self.place(t)] = total(m.g)

    def end(self, t):
        n = len(self.m.offsets)
        for o in range(n):
            self.far[t, o].wait_recv()
        value = self.acc[self.place(t)]
        for o in range(n):
            value = value + self.rg[t, o].astype(F32)
        self.acc[self.place(t)] = value

    def finish(self):
        for copy in list(self.pair.values()) + list(self.far.values()):
            copy.wait_send()


def flat(v):
    return v.reshape(-1, v.shape[-1])


def dot(a, b, ca, cb):
    return lax.dot_general(a, b, (((ca,), (cb,)), ((), ())), preferred_element_type=F32)


def unit_scale(v):
    return lax.rsqrt(jnp.mean(v * v, axis=-1, keepdims=True) + eps)


def kernel(sizes, D, nw, *refs):
    ws, refs = refs[:nw], refs[nw:]
    (x_late, x_early, cot, pre_gain, post_gain, y_out, dx_out, owned_out,
     wout, xout, dpost, gate, up, hid, hout, p, rx, tx, rg, acc, dall, dhid, dgate, dup, dz,
           q, qx, qt, qg, dacc, dw, sems) = refs
    m = Grid(sizes)
    cp = Copies(sems)
    n, fy, tp, fz = len(m.offsets), m.fy, m.tp, m.fz
    m.barrier(group=True, pair=True, levels=True)
    f = m.z * fy + m.y
    rows, part = x_late.shape[0], wout.shape[-1]
    ce, drows = rows // tp, D // m.fs

    def weight(g, i):
        if nw == 1:
            return ws[0].at[g, i]
        return ws[i].at[:, pl.ds(pl.multiple_of(g * part, part), part)]

    def owned_at(g):
        if nw == 1:
            return owned_out.at[g]
        return owned_out.at[:, pl.ds(pl.multiple_of(g * part, part), part)]

    def columns(block):
        return slice(block * drows, (block + 1) * drows)

    def where(z, c):
        e, i = c
        return wout.at[i, z * fy + lax.rem(m.y + e, fy)]

    def first(c):
        return weight(m.g, c[1]) if c[0] == 0 else where(m.z, c)

    ys = {}

    def trade(i):
        for e in range(1, fy):
            o = m.offsets.index((0, e))
            ys[e, i] = cp.push(weight(m.index(o), i), wout.at[i, f], m.peer(o))

    ring_a = Ring(m, cp, first, where, [(e, i) for i in (0, 1) for e in range(fy)])
    ring_b = Ring(m, cp, first, where, [(e, 2) for e in range(fy)])
    trade(0)
    trade(1)
    for i in (0, 1):
        ring_a.send(0, 1, (0, i))
        ring_a.send(1, 1, (0, 1 - i))
    for t in range(tp):
        for place, ref in ((0, x_late), (ce, x_early)):
            v = ref[t * ce:(t + 1) * ce].astype(F32)
            v = (v * unit_scale(v) * pre_gain[...]).astype(BF16)
            for block in range(m.fs):
                xout[m.g, t, block, place:place + ce] = v[:, columns(block)]
    for i in range(3):
        wout[i, f] = weight(m.g, i)[...]
    xs = {o: cp.push(xout.at[m.g, m.k], xout.at[m.g, m.k], m.peer(o)) for o in range(n)}
    trade(2)
    mine = pl.ds(pl.multiple_of(m.k * ce, ce), ce)
    v = 0.5 * cot[mine].astype(F32) * post_gain[...]
    for block in range(m.fs):
        dpost[block] = v[:, columns(block)]
    for e in range(1, fy):
        back = (fy - e) % fy
        for i in (0, 1):
            ys[back, i].wait_recv()
        for i in (0, 1):
            ring_a.send(0, 1, (e, i))
            ring_a.send(1, 1, (e, 1 - i))
    for i in (0, 1):
        ring_a.arrive(0, 1, (0, i))
        ring_a.arrive(1, 1, (0, 1 - i))
    passed = []

    def spread(copies, out):
        for o in copies:
            copies[o].wait_recv()
            src = m.index(o, -1)
            for j in range(1, tp):
                passed.append(cp.push(out.at[src, m.k], out.at[src, m.k], m.sibling(j)))

    spread(xs, xout)
    ring_a.step(1)
    for e in range(fy):
        if e:
            ys[(fy - e) % fy, 2].wait_recv()
        for d in (0, 1):
            ring_b.send(d, 1, (e, 2))
    for copy in passed:
        copy.wait()
    passed.clear()

    gate[...] = jnp.zeros_like(gate)
    up[...] = jnp.zeros_like(up)
    for dist, s, ds in stages(m):
        for d in ds:
            ring_a.step(s, (d,))
        zt = m.along(dist)
        for e in range(fy):
            block = zt * fy + e

            def add(i, carry, block=block):
                rows = flat(xout[i, :, block])
                gate[i] += dot(rows, wout[0, block], 1, 0)
                up[i] += dot(rows, wout[1, block], 1, 0)
                return carry

            lax.fori_loop(0, m.G, add, 0)

    def activate(i, carry):
        v = gate[i]
        hid[i] = (v * (1.0 / (1.0 + jnp.exp(-v))) * up[i]).astype(BF16)
        return carry

    lax.fori_loop(0, m.G, activate, 0)
    for t in range(tp):
        hout[m.z, t] = hid[:, (2 * t + 1) * ce:(2 * t + 2) * ce]
    ring_h = Ring(m, cp, lambda c: hout.at[m.z, c], lambda z, c: hout.at[z, c], list(range(tp)))

    order = stages(m)
    sc = Scatter(m, cp, p, rx, tx, rg, acc, lambda t: m.along(order[t][0]))
    for t, (dist, s, ds) in enumerate(order):
        for d in ds:
            ring_b.step(s, (d,))
        if t == len(order) - 1:
            for i in range(tp):
                for d in (0, 1):
                    ring_h.send(d, 1, ring_h.order[d][i])
        zt = m.along(dist)
        for e in range(fy):
            block = zt * fy + e

            def product(i, carry, block=block, e=e):
                p[t, e, i] = dot(hid[i], wout[2, block], 1, 1).astype(BF16).reshape(p.shape[3:])
                return carry

            lax.fori_loop(0, m.G, product, 0)
        sc.start(t)
        if t:
            sc.middle(t - 1)
    sc.middle(len(order) - 1)
    for t in range(len(order)):
        sc.end(t)
    places = [divmod(block, fy) for block in range(m.fs)]

    def row_sum(term):
        return sum(jnp.sum(term(*place), axis=-1, keepdims=True) for place in places)

    rz = lax.rsqrt(row_sum(lambda t, e: acc[t, e, ce:] * acc[t, e, ce:]) / D + eps)
    mix = row_sum(lambda t, e: acc[t, e, ce:] * dpost[t * fy + e]) / D
    factor = rz * rz * mix
    for t, e in places:
        dall[m.g, m.k, t * fy + e] = (rz * (dpost[t * fy + e] - acc[t, e, ce:] * factor)).astype(BF16)
    dg = {o: cp.push(dall.at[m.g, m.k], dall.at[m.g, m.k], m.peer(o)) for o in range(n)}
    own = [cp.push(dall.at[m.g, m.k], dall.at[m.g, m.k], m.sibling(j)) for j in range(1, tp)]
    ring_h.step(1)
    late_rz = lax.rsqrt(row_sum(lambda t, e: acc[t, e, :ce] * acc[t, e, :ce]) / D + eps)
    for t, e in places:
        cols = columns(t * fy + e)
        v = 0.5 * acc[t, e, :ce] * late_rz * post_gain[:, cols]
        y_out[m.k, :, cols] = (x_late[mine, cols].astype(F32) + v).astype(BF16)
    spread(dg, dall)
    late = [cp.push(y_out.at[m.k], y_out.at[m.k], m.sibling(j)) for j in range(1, tp)]
    across = {}
    for s in range(1, fz):
        src = dall.at[:, m.k, pl.ds(m.along(s) * fy, fy)]
        across[s] = cp.push(src, dz.at[m.z, m.k], m.level(s))
    for copy in passed + own:
        copy.wait()
    passed.clear()

    def back(i, carry):
        total = dot(flat(dall[i, :, 0]), wout[2, 0], 1, 0)
        for block in range(1, m.fs):
            total = total + dot(flat(dall[i, :, block]), wout[2, block], 1, 0)
        dhid[i] = total
        return carry

    lax.fori_loop(0, m.G, back, 0)

    def gates(i, carry):
        for t in range(tp):
            its, to = pl.ds((2 * t + 1) * ce, ce), pl.ds(t * ce, ce)
            g, dh = gate[i, its], dhid[i, to]
            sig = 1.0 / (1.0 + jnp.exp(-g))
            dgate[i, to] = (dh * up[i, its] * sig * (1.0 + g * (1.0 - sig))).astype(BF16)
            dup[i, to] = (dh * g * sig).astype(BF16)
        return carry

    lax.fori_loop(0, m.G, gates, 0)
    dsc = Scatter(m, cp, q, qx, qt, qg, dacc, lambda t: t)
    for t in range(fz):
        for e in range(fy):
            block = t * fy + e

            def terms(i, carry, block=block, e=e, t=t):
                v = dot(dgate[i], wout[0, block], 1, 1) + dot(dup[i], wout[1, block], 1, 1)
                q[t, e, i] = v.astype(BF16).reshape(q.shape[3:])
                return carry

            lax.fori_loop(0, m.G, terms, 0)
        dsc.start(t)
        if t:
            dsc.middle(t - 1)
    dsc.middle(fz - 1)
    for s in range(2, ring_h.half + 1):
        ring_h.step(s)
    dz[m.z] = jnp.stack([dall[:, t, pl.ds(m.z * fy, fy)] for t in range(tp)])
    for s in across:
        across[s].wait_recv()
        src = m.along(-s)
        for j in range(1, tp):
            passed.append(cp.push(dz.at[src, m.k], dz.at[src, m.k], m.sibling(j)))
    for t in range(fz):
        dsc.end(t)
    xf = x_early[mine].astype(F32)
    rs = unit_scale(xf)
    gained = lambda t, e: dacc[t, e] * pre_gain[:, columns(t * fy + e)]
    mix = row_sum(lambda t, e: gained(t, e) * xf[:, columns(t * fy + e)]) / D
    factor = rs * rs * mix
    for t, e in places:
        cols = columns(t * fy + e)
        v = rs * (gained(t, e) - xf[:, cols] * factor)
        dx_out[m.k, :, cols] = (cot[mine, cols].astype(F32) + v).astype(BF16)
    last = [cp.push(dx_out.at[m.k], dx_out.at[m.k], m.sibling(j)) for j in range(1, tp)]
    for copy in passed:
        copy.wait()
    sends = []

    def gradient(r, e):
        a = dz[:, :, pl.ds(r * fy, fy), e]
        b = hout[:, :, pl.ds(r * fy, fy)]
        return dot(flat(a), flat(b), 0, 0).astype(BF16)

    for o in range(n):
        r, y = m.moved(o)
        dw[o] = gradient(r, y)
        sends.append(cp.push(dw.at[o], owned_at(m.g), m.peer(o)))
    owned_at(m.g)[...] = gradient(m.r, m.y)
    for copy in sends + last + late:
        copy.wait()
    for copies in (xs, ys, dg, across):
        for copy in copies.values():
            copy.wait_send()
    for thing in (ring_a, ring_b, ring_h, sc, dsc):
        thing.finish()


def body(sizes, x_late, x_early, cotangent, pre_gain, post_gain, gate_weight, up_weight, down_weight,
         down_grad_sum):
    R, fs, tp = sizes
    fy = 2
    fz, G = fs // fy, R * fy
    rows, D = x_late.shape
    drows, width = gate_weight.shape
    part = width // G
    n = G - 1
    ce = rows // tp
    c = 2 * ce
    S, V = jax.ShapeDtypeStruct, pltpu.VMEM

    weights = [gate_weight, up_weight, down_weight]
    aligned = part % 128 == 0
    if not aligned:
        weights = [jnp.stack([w.reshape(drows, G, part) for w in weights]).transpose(2, 0, 1, 3)]
    ring = 2 * (fz // 2)
    count = (3 * (fy - 1) + ring * (3 * fy + tp) + 2 * (n + n * (tp - 1)) + 3 * (tp - 1)
             + 2 * fz * (tp - 1 + n) + (fz - 1) * tp + n)

    def scatter(c):
        return [
            V((fz, fy, G, tp, c, drows), BF16),
            V((tp - 1, fz, fy, G, c, drows), BF16),
            V((fz, n, fy, c, drows), BF16),
            V((fz, n, fy, c, drows), BF16),
            V((fz, fy, c, drows), F32),
        ]

    all_rows, early_rows = tp * c, tp * ce
    y_late, dx_early, owned = pl.pallas_call(
        functools.partial(kernel, sizes, D, len(weights)),
        out_shape=[
            S((tp, ce, D), BF16), S((tp, ce, D), BF16),
            S((drows, width) if aligned else (G, drows, part), BF16),
        ],
        in_specs=[VMEM] * (len(weights) + 5),
        out_specs=[VMEM] * 3,
        scratch_shapes=[
            V((3, fs, drows, part), BF16),
            V((G, tp, fs, c, drows), BF16),
            V((fs, ce, drows), F32),
            V((G, all_rows, part), F32),
            V((G, all_rows, part), F32),
            V((G, all_rows, part), BF16),
            V((fz, tp, G, ce, part), BF16),
        ] + scatter(c) + [
            V((G, tp, fs, ce, drows), BF16),
            V((G, early_rows, part), F32),
            V((G, early_rows, part), BF16),
            V((G, early_rows, part), BF16),
            V((fz, tp, G, fy, ce, drows), BF16),
        ] + scatter(ce) + [
            V((n, drows, part), BF16),
            DMA((2, count)),
        ],
        compiler_params=pltpu.CompilerParams(
            collective_id=0, has_side_effects=True, vmem_limit_bytes=60 * 1024 * 1024
        ),
    )(*weights, x_late, x_early, cotangent, pre_gain.reshape(1, D), post_gain.reshape(1, D))
    if not aligned:
        owned = owned.transpose(1, 0, 2).reshape(drows, width)
    down_grad_out = down_grad_sum + owned.astype(F32)
    return (y_late.reshape(rows, D), dx_early.reshape(rows, D), down_grad_out)


def solution(mesh):
    sizes = tuple(mesh.shape[a] for a in ("rep", "fs", "tp"))
    in_specs = (
        P(("rep", "fs"), None),
        P(("rep", "fs"), None),
        P(("rep", "fs"), None),
        P(),
        P(),
        P("fs", "tp"),
        P("fs", "tp"),
        P("fs", "tp"),
        P(("rep", "fs"), "tp"),
    )
    out_specs = (P(("rep", "fs"), None), P(("rep", "fs"), None), P(("rep", "fs"), "tp"))
    return jax.shard_map(
        functools.partial(body, sizes), mesh=mesh, in_specs=in_specs, out_specs=out_specs, check_vma=False
    )
```

profile of v0, /device:TPU:0, one launch (start us, length us, event | category | flops | bytes accessed | tf_op | source)
XLA Modules:
  0.0 153.9 jit_solution(6591694985172417746)
XLA Ops:
  0.6 0.0 copy-start
  0.6 149.0 %shard_map.112 = (bf16[2,64,2048]{2,1,0:T(8,128)(2,1)}, bf16[2,64,2048]{2,1,0:T(8,128)(2,1)}, bf16[256,1536]{1,0:T(8,128)(2,1)}) custom-call(bf16[256,1536]{1,0:T(8,128)(2,1)} %refs_0_.1, bf16[256,1536]{1,0:T(8,128)(2,1)} %refs_1_.1, bf16[256,1536]{1,0:T(8,128)(2,1)} %refs_2_.1, bf16[128,2048]{1,0:T(8,128)(2,1)} %refs_3_.1, bf16[128,2048]{1,0:T(8,128)(2,1)} %refs_4_.1, ...), custom_call_target="tpu_custom_call" | custom-call | tf_op jit(solution)/shard_map/pallas_call | solution.py:456
  149.7 0.0 copy-done
  149.7 0.0 copy-start.2
  149.7 0.0 copy-start.1
  149.7 2.6 %convert_add_fusion = f32[256,1536]{1,0:T(8,128)} fusion(f32[256,1536]{1,0:T(8,128)S(1)} %copy-done, bf16[256,1536]{1,0:T(8,128)(2,1)} %get-tuple-element.8), kind=kLoop, calls=%fused_computation | loop fusion | flops 786432 | bytes 3932160 | tf_op jit(solution)/shard_map/add | solution.py:488
  152.3 0.0 copy-done.2
  152.3 0.8 copy.14
  153.1 0.0 copy-done.1
  153.1 0.8 copy.15
Async XLA Ops:
  0.6 149.1 %copy-start = (f32[256,1536]{1,0:T(8,128)S(1)}, f32[256,1536]{1,0:T(8,128)}, u32[]{:S(2)}) copy-start(f32[256,1536]{1,0:T(8,128)} %param.17) | copy-start | bytes 4718596
  149.7 2.6 %copy-start.2 = (bf16[2,64,2048]{2,1,0:T(8,128)(2,1)S(1)}, bf16[2,64,2048]{2,1,0:T(8,128)(2,1)}, u32[]{:S(2)}) copy-start(bf16[2,64,2048]{2,1,0:T(8,128)(2,1)} %get-tuple-element.6) | copy-start | bytes 1572868
  149.7 3.4 %copy-start.1 = (bf16[2,64,2048]{2,1,0:T(8,128)(2,1)S(1)}, bf16[2,64,2048]{2,1,0:T(8,128)(2,1)}, u32[]{:S(2)}) copy-start(bf16[2,64,2048]{2,1,0:T(8,128)(2,1)} %get-tuple-element.7) | copy-start | bytes 1572868
where the time goes:
time: 157 us; the launch traced here: 154 us
  Pallas kernels  149 us (95%)
  other arithmetic  2.55 us (2%)
  local copies, waits for them, and re-layouts  1.6 us (1%)
    pallas_call x1, Pallas kernels, body(): pl.pallas_call(functools.partial(kernel, sizes, D, len(weights)), out_sha...  149 us

commit v1 on v0

--- a/solution.py
+++ b/solution.py
@@ -19,10 +19,12 @@
         self.R, self.fs, self.tp = sizes
         self.fy = 2
         self.fz = self.fs // self.fy
+        self.H = self.fz // 2
         self.G = self.R * self.fy
         self.offsets = list(itertools.product(range(self.R), range(self.fy)))[1:]
-        self.r, f, self.k = (lax.axis_index(n) for n in ("rep", "fs", "tp"))
-        self.z, self.y = lax.div(f, self.fy), lax.rem(f, self.fy)
+        self.r, self.f, self.k = (lax.axis_index(n) for n in ("rep", "fs", "tp"))
+        self.h, self.y, self.b = lax.div(self.f, 4), lax.rem(lax.div(self.f, 2), 2), lax.rem(self.f, 2)
+        self.z = self.h * 2 + self.b
         self.g = self.r * self.fy + self.y
 
     def moved(self, o, sign=1):
@@ -35,33 +37,37 @@
         r, y = self.moved(o, sign)
         return r * self.fy + y
 
+    def device(self, r, z, y):
+        return {"rep": r, "fs": lax.div(z, 2) * 4 + y * 2 + lax.rem(z, 2), "tp": self.k}
+
     def peer(self, o):
         r, y = self.moved(o)
-        return {"rep": r, "fs": self.z * self.fy + y, "tp": self.k}
+        return self.device(r, self.z, y)
 
     def sibling_index(self, j):
         return lax.rem(self.k + j, self.tp)
 
     def sibling(self, j):
-        return {"rep": self.r, "fs": self.z * self.fy + self.y, "tp": self.sibling_index(j)}
-
-    def along(self, step):
-        return lax.rem(self.z + self.fz + step, self.fz)
-
-    def level(self, step):
-        return {"rep": self.r, "fs": self.along(step) * self.fy + self.y, "tp": self.k}
-
-    def barrier(self, group=False, pair=False, ring=False, levels=False):
+        return {"rep": self.r, "fs": self.f, "tp": self.sibling_index(j)}
+
+    def up(self, dh):
+        return lax.rem(self.h + self.H + dh, self.H)
+
+    def along(self, dh, db):
+        return self.up(dh) * 2 + lax.rem(self.b + db, 2)
+
+    def level(self, dh, db):
+        return self.device(self.r, self.along(dh, db), self.y)
+
+    def across(self, dh, dy):
+        return self.device(self.r, self.along(dh, 0), lax.rem(self.y + dy, self.fy))
+
+    def barrier(self):
         sem = pltpu.get_barrier_semaphore()
-        targets = []
-        if group:
-            targets += [self.peer(o) for o in range(len(self.offsets))]
-        if pair:
-            targets += [self.sibling(j) for j in range(1, self.tp)]
-        if levels:
-            targets += [self.level(s) for s in range(1, self.fz)]
-        elif ring:
-            targets += [self.level(1), self.level(-1)]
+        targets = [self.peer(o) for o in range(len(self.offsets))]
+        targets += [self.sibling(j) for j in range(1, self.tp)]
+        targets += [self.across(dh, dy) for dh in range(1, self.H) for dy in range(self.fy)]
+        targets += [self.level(dh, 1) for dh in range(self.H)]
         for t in targets:
             pl.semaphore_signal(sem, inc=1, device_id=t, device_id_type=pl.DeviceIdType.MESH)
         pl.semaphore_wait(sem, len(targets))
@@ -69,56 +75,112 @@
 
 class Copies:
     def __init__(self, sems):
-        self.sems, self.used = sems, 0
-
-    def push(self, src, dst, to):
-        copy = pltpu.make_async_remote_copy(
-            src_ref=src, dst_ref=dst, send_sem=self.sems.at[0, self.used], recv_sem=self.sems.at[1, self.used],
+        self.sems, self.used, self.open = sems, 0, []
+
+    def make(self, src, dst, to, send=None, recv=None):
+        if send is None:
+            send = recv = self.used
+            self.used += 1
+        return pltpu.make_async_remote_copy(
+            src_ref=src, dst_ref=dst, send_sem=self.sems.at[0, send], recv_sem=self.sems.at[1, recv],
             device_id=to, device_id_type=pl.DeviceIdType.MESH,
         )
-        self.used += 1
+
+    def push(self, src, dst, to):
+        copy = self.make(src, dst, to)
         copy.start()
         return copy
 
-
-class Ring:
-    def __init__(self, m, cp, first, slot, chunks):
-        self.m, self.cp, self.first, self.slot = m, cp, first, slot
-        self.order = {0: chunks, 1: chunks[len(chunks) // 2:] + chunks[:len(chunks) // 2]}
-        self.fronts = {0: set(chunks[: len(chunks) // 2]), 1: set(chunks[len(chunks) // 2:])}
-        self.half = m.fz // 2
-        self.sent, self.arrived = {}, set()
-
-    def send(self, d, s, c):
-        sign = 1 if d == 0 else -1
-        block = self.m.along(-sign * (s - 1))
-        src = self.first(c) if s == 1 else self.slot(block, c)
-        self.sent[d, s, c] = self.cp.push(src, self.slot(block, c), self.m.level(sign))
-
-    def arrive(self, d, s, c):
-        if (d, s, c) not in self.sent or (d, s, c) in self.arrived:
-            return
-        self.sent[d, s, c].wait_recv()
-        self.arrived.add((d, s, c))
-        if s + 1 < self.half or (s + 1 == self.half and c in self.fronts[d]):
-            self.send(d, s + 1, c)
-
-    def step(self, s, ds=(0, 1)):
-        for i in range(len(self.order[0])):
-            for d in ds:
-                self.arrive(d, s, self.order[d][i])
+    def later(self, src, dst, to):
+        copy = self.push(src, dst, to)
+        self.open.append(copy)
+        return copy
 
     def finish(self):
-        for copy in self.sent.values():
+        for copy in self.open:
             copy.wait_send()
 
 
-def stages(m):
-    half = m.fz // 2
-    out = [(0, 0, ())]
-    for s in range(1, half):
-        out += [(-s, s, (0,)), (s, s, (1,))]
-    return out + [(half, half, (0, 1))]
+class Weights:
+    def __init__(self, m, cp, weight, wout):
+        self.m, self.cp, self.weight, self.wout = m, cp, weight, wout
+        self.pair, self.far, self.slot, self.over = {}, {}, {}, {}
+        for i in range(3):
+            for dh in range(1, m.H):
+                base = cp.used
+                cp.used += m.fy
+                for dy in range(m.fy):
+                    g = m.r * m.fy + lax.rem(m.y + dy, m.fy)
+                    copy = cp.make(weight(g, i), wout.at[i, self.block(m.z, m.y)], m.across(dh, dy),
+                                   base + dy, base + m.y)
+                    cp.open.append(copy)
+                    self.far[dh, dy, i] = copy
+                self.slot[dh, i] = base
+
+    def block(self, z, y):
+        return z * self.m.fy + y
+
+    def near(self, dh):
+        return jnp.where(self.m.up(dh) > self.m.h, 1, 0) == self.m.y
+
+    def cross(self, ii, near):
+        m = self.m
+        for dh in range(1, m.H):
+            @pl.when(self.near(dh) == near)
+            def _():
+                for i in ii:
+                    for dy in range(m.fy):
+                        self.far[dh, dy, i].start()
+
+    def trade(self, ii):
+        m = self.m
+        for i in ii:
+            y = lax.rem(m.y + 1, m.fy)
+            dst = self.wout.at[i, self.block(m.z, m.y)]
+            self.pair[i] = self.cp.later(self.weight(m.r * m.fy + y, i), dst, m.across(0, 1))
+
+    def pass_on(self, key, src, z, y):
+        self.over[key] = self.cp.later(src, self.wout.at[key[-1], self.block(z, y)], self.m.level(0, 1))
+
+    def own(self, ii):
+        for i in ii:
+            self.pass_on(("own", i), self.weight(self.m.g, i), self.m.z, self.m.y)
+
+    def traded(self, ii):
+        m = self.m
+        y = lax.rem(m.y + 1, m.fy)
+        for i in ii:
+            self.pair[i].wait_recv()
+            self.pass_on(("pair", i), self.wout.at[i, self.block(m.z, y)], m.z, y)
+
+    def source(self, dh, near):
+        m = self.m
+        y = jnp.where(m.up(-dh) < m.h, 1, 0)
+        return m.along(-dh, 0), y if near else 1 - y
+
+    def crossed(self, ii, near):
+        m = self.m
+        for dh in range(1, m.H):
+            z, y = self.source(dh, near)
+            for i in ii:
+                ref = self.wout.at[i, self.block(z, y)]
+                base = self.slot[dh, i]
+                self.cp.make(ref, ref, m.across(dh, 0), base, base + y).wait_recv()
+                self.pass_on((dh, near, i), ref, z, y)
+
+    def landed(self, key):
+        self.over[key].wait_recv()
+
+    def steps(self):
+        m = self.m
+        out = [("own", m.z, m.y), ("pair", m.z, lax.rem(m.y + 1, m.fy))]
+        for near in (True, False):
+            out += [((dh, near),) + self.source(dh, near) for dh in range(1, m.H)]
+        return out
+
+
+def levels(m):
+    return [(dh, db) for dh in range(m.H) for db in range(2)]
 
 
 class Scatter:
@@ -183,8 +245,7 @@
     m = Grid(sizes)
     cp = Copies(sems)
     n, fy, tp, fz = len(m.offsets), m.fy, m.tp, m.fz
-    m.barrier(group=True, pair=True, levels=True)
-    f = m.z * fy + m.y
+    m.barrier()
     rows, part = x_late.shape[0], wout.shape[-1]
     ce, drows = rows // tp, D // m.fs
 
@@ -199,89 +260,89 @@
         return owned_out.at[:, pl.ds(pl.multiple_of(g * part, part), part)]
 
     def columns(block):
-        return slice(block * drows, (block + 1) * drows)
-
-    def where(z, c):
-        e, i = c
-        return wout.at[i, z * fy + lax.rem(m.y + e, fy)]
-
-    def first(c):
-        return weight(m.g, c[1]) if c[0] == 0 else where(m.z, c)
-
-    ys = {}
-
-    def trade(i):
-        for e in range(1, fy):
-            o = m.offsets.index((0, e))
-            ys[e, i] = cp.push(weight(m.index(o), i), wout.at[i, f], m.peer(o))
-
-    ring_a = Ring(m, cp, first, where, [(e, i) for i in (0, 1) for e in range(fy)])
-    ring_b = Ring(m, cp, first, where, [(e, 2) for e in range(fy)])
-    trade(0)
-    trade(1)
-    for i in (0, 1):
-        ring_a.send(0, 1, (0, i))
-        ring_a.send(1, 1, (0, 1 - i))
+        z, y = divmod(block, fy)
+        f = (z // 2) * 4 + y * 2 + z % 2
+        return slice(f * drows, (f + 1) * drows)
+
+    both, third = (0, 1), (2,)
+    w = Weights(m, cp, weight, wout)
+    w.cross(both, True)
+    w.trade(both)
+    w.own(both)
     for t in range(tp):
         for place, ref in ((0, x_late), (ce, x_early)):
             v = ref[t * ce:(t + 1) * ce].astype(F32)
             v = (v * unit_scale(v) * pre_gain[...]).astype(BF16)
             for block in range(m.fs):
                 xout[m.g, t, block, place:place + ce] = v[:, columns(block)]
+    side = [o for o in range(n) if m.offsets[o][1] == 0]
+    beside = m.offsets.index((0, 1))
+    mine_x = xout.at[m.g, m.k]
+    xz = cp.later(mine_x, mine_x, m.peer(beside))
+    xs = {o: cp.later(mine_x, mine_x, m.peer(o)) for o in side}
+    w.cross(both, False)
+    w.cross(third, True)
+    w.trade(third)
+    w.cross(third, False)
     for i in range(3):
-        wout[i, f] = weight(m.g, i)[...]
-    xs = {o: cp.push(xout.at[m.g, m.k], xout.at[m.g, m.k], m.peer(o)) for o in range(n)}
-    trade(2)
+        wout[i, w.block(m.z, m.y)] = weight(m.g, i)[...]
     mine = pl.ds(pl.multiple_of(m.k * ce, ce), ce)
     v = 0.5 * cot[mine].astype(F32) * post_gain[...]
     for block in range(m.fs):
         dpost[block] = v[:, columns(block)]
-    for e in range(1, fy):
-        back = (fy - e) % fy
-        for i in (0, 1):
-            ys[back, i].wait_recv()
-        for i in (0, 1):
-            ring_a.send(0, 1, (e, i))
-            ring_a.send(1, 1, (e, 1 - i))
-    for i in (0, 1):
-        ring_a.arrive(0, 1, (0, i))
-        ring_a.arrive(1, 1, (0, 1 - i))
     passed = []
+
+    def share(out, g):
+        for j in range(1, tp):
+            passed.append(cp.push(out.at[g, m.k], out.at[g, m.k], m.sibling(j)))
 
     def spread(copies, out):
         for o in copies:
             copies[o].wait_recv()
-            src = m.index(o, -1)
-            for j in range(1, tp):
-                passed.append(cp.push(out.at[src, m.k], out.at[src, m.k], m.sibling(j)))
-
+            share(out, m.index(o, -1))
+
+    w.traded(both)
+    w.own(third)
     spread(xs, xout)
-    ring_a.step(1)
-    for e in range(fy):
-        if e:
-            ys[(fy - e) % fy, 2].wait_recv()
-        for d in (0, 1):
-            ring_b.send(d, 1, (e, 2))
+    w.crossed(both, True)
+    xz.wait_recv()
+    other = m.index(beside, -1)
+    xf = {o: cp.later(xout.at[other, m.k], xout.at[other, m.k], m.peer(o)) for o in side}
+    share(xout, other)
+    w.crossed(third, True)
+    for o in side:
+        xf[o].wait_recv()
+        r, _ = m.moved(o, -1)
+        share(xout, r * fy + lax.rem(m.y + 1, fy))
     for copy in passed:
         copy.wait()
     passed.clear()
 
     gate[...] = jnp.zeros_like(gate)
     up[...] = jnp.zeros_like(up)
-    for dist, s, ds in stages(m):
-        for d in ds:
-            ring_a.step(s, (d,))
-        zt = m.along(dist)
-        for e in range(fy):
-            block = zt * fy + e
-
-            def add(i, carry, block=block):
-                rows = flat(xout[i, :, block])
-                gate[i] += dot(rows, wout[0, block], 1, 0)
-                up[i] += dot(rows, wout[1, block], 1, 0)
-                return carry
-
-            lax.fori_loop(0, m.G, add, 0)
+
+    def grow(block):
+        def add(i, carry):
+            rows = flat(xout[i, :, block])
+            gate[i] += dot(rows, wout[0, block], 1, 0)
+            up[i] += dot(rows, wout[1, block], 1, 0)
+            return carry
+
+        lax.fori_loop(0, m.G, add, 0)
+
+    def twin(z):
+        return lax.div(z, 2) * 2 + 1 - lax.rem(z, 2)
+
+    steps = w.steps()
+    first_far = 1 + m.H
+    for s, (key, z, y) in enumerate(steps):
+        key = key if isinstance(key, tuple) else (key,)
+        if s == first_far:
+            w.crossed(both, False)
+        grow(w.block(z, y))
+        for i in both:
+            w.landed(key + (i,))
+        grow(w.block(twin(z), y))
 
     def activate(i, carry):
         v = gate[i]
@@ -291,18 +352,24 @@
     lax.fori_loop(0, m.G, activate, 0)
     for t in range(tp):
         hout[m.z, t] = hid[:, (2 * t + 1) * ce:(2 * t + 2) * ce]
-    ring_h = Ring(m, cp, lambda c: hout.at[m.z, c], lambda z, c: hout.at[z, c], list(range(tp)))
-
-    order = stages(m)
-    sc = Scatter(m, cp, p, rx, tx, rg, acc, lambda t: m.along(order[t][0]))
-    for t, (dist, s, ds) in enumerate(order):
-        for d in ds:
-            ring_b.step(s, (d,))
-        if t == len(order) - 1:
-            for i in range(tp):
-                for d in (0, 1):
-                    ring_h.send(d, 1, ring_h.order[d][i])
-        zt = m.along(dist)
+    w.traded(third)
+    order = levels(m)
+    sc = Scatter(m, cp, p, rx, tx, rg, acc, lambda t: m.along(*order[t]))
+    hs, hf = {}, {}
+    for t, (dh, db) in enumerate(order):
+        if t == 1:
+            w.landed(("own", 2))
+            w.landed(("pair", 2))
+        if t == 2:
+            w.crossed(third, False)
+            for c in range(tp):
+                for d in range(1, m.H):
+                    hs[d, c] = cp.later(hout.at[m.z, c], hout.at[m.z, c], m.level(d, 0))
+                hf[0, c] = cp.later(hout.at[m.z, c], hout.at[m.z, c], m.level(0, 1))
+        if t > 2 and db == 1:
+            for near in (True, False):
+                w.landed(((m.H - dh) % m.H, near, 2))
+        zt = m.along(dh, db)
         for e in range(fy):
             block = zt * fy + e
 
@@ -329,7 +396,10 @@
         dall[m.g, m.k, t * fy + e] = (rz * (dpost[t * fy + e] - acc[t, e, ce:] * factor)).astype(BF16)
     dg = {o: cp.push(dall.at[m.g, m.k], dall.at[m.g, m.k], m.peer(o)) for o in range(n)}
     own = [cp.push(dall.at[m.g, m.k], dall.at[m.g, m.k], m.sibling(j)) for j in range(1, tp)]
-    ring_h.step(1)
+    for d, c in hs:
+        hs[d, c].wait_recv()
+        ref = hout.at[m.along(-d, 0), c]
+        hf[d, c] = cp.later(ref, ref, m.level(0, 1))
     late_rz = lax.rsqrt(row_sum(lambda t, e: acc[t, e, :ce] * acc[t, e, :ce]) / D + eps)
     for t, e in places:
         cols = columns(t * fy + e)
@@ -338,9 +408,9 @@
     spread(dg, dall)
     late = [cp.push(y_out.at[m.k], y_out.at[m.k], m.sibling(j)) for j in range(1, tp)]
     across = {}
-    for s in range(1, fz):
-        src = dall.at[:, m.k, pl.ds(m.along(s) * fy, fy)]
-        across[s] = cp.push(src, dz.at[m.z, m.k], m.level(s))
+    for s in order[1:]:
+        src = dall.at[:, m.k, pl.ds(m.along(*s) * fy, fy)]
+        across[s] = cp.later(src, dz.at[m.z, m.k], m.level(*s))
     for copy in passed + own:
         copy.wait()
     passed.clear()
@@ -379,12 +449,12 @@
         if t:
             dsc.middle(t - 1)
     dsc.middle(fz - 1)
-    for s in range(2, ring_h.half + 1):
-        ring_h.step(s)
+    for copy in hf.values():
+        copy.wait_recv()
     dz[m.z] = jnp.stack([dall[:, t, pl.ds(m.z * fy, fy)] for t in range(tp)])
     for s in across:
         across[s].wait_recv()
-        src = m.along(-s)
+        src = m.along(-s[0], s[1])
         for j in range(1, tp):
             passed.append(cp.push(dz.at[src, m.k], dz.at[src, m.k], m.sibling(j)))
     for t in range(fz):
@@ -415,10 +485,10 @@
     owned_at(m.g)[...] = gradient(m.r, m.y)
     for copy in sends + last + late:
         copy.wait()
-    for copies in (xs, ys, dg, across):
-        for copy in copies.values():
-            copy.wait_send()
-    for thing in (ring_a, ring_b, ring_h, sc, dsc):
+    for copy in dg.values():
+        copy.wait_send()
+    cp.finish()
+    for thing in (sc, dsc):
         thing.finish()
 
 
@@ -439,8 +509,7 @@
     aligned = part % 128 == 0
     if not aligned:
         weights = [jnp.stack([w.reshape(drows, G, part) for w in weights]).transpose(2, 0, 1, 3)]
-    ring = 2 * (fz // 2)
-    count = (3 * (fy - 1) + ring * (3 * fy + tp) + 2 * (n + n * (tp - 1)) + 3 * (tp - 1)
+    count = (3 * (2 * fz - 1) + fz * tp + 2 * (n + n * (tp - 1)) + 3 * (tp - 1)
              + 2 * fz * (tp - 1 + n) + (fz - 1) * tp + n)
 
     def scatter(c):

time: 157 us -> 188 us (1.20); the launches traced: 154 us -> 188 us
  Pallas kernels: 149 us -> 183 us
    pallas_call x1, Pallas kernels: 149 us -> 183 us  [body(): pl.pallas_call(functools.partial(kernel, sizes, D, len(weights)), out_sha...]
where the time goes in v1:
time: 188 us
  Pallas kernels  183 us (97%)
  other arithmetic  2.55 us (1%)
    pallas_call x1, Pallas kernels, body(): pl.pallas_call(functools.partial(kernel, sizes, D, len(weights)), out_sha...  183 us

profile of v1, /device:TPU:0, one launch (start us, length us, event | category | flops | bytes accessed | tf_op | source)
XLA Modules:
  0.0 188.3 jit_solution(13282988527272494236)
XLA Ops:
  0.6 0.0 copy-start
  0.6 183.5 %shard_map.112 = (bf16[2,64,2048]{2,1,0:T(8,128)(2,1)}, bf16[2,64,2048]{2,1,0:T(8,128)(2,1)}, bf16[256,1536]{1,0:T(8,128)(2,1)}) custom-call(bf16[256,1536]{1,0:T(8,128)(2,1)} %refs_0_.1, bf16[256,1536]{1,0:T(8,128)(2,1)} %refs_1_.1, bf16[256,1536]{1,0:T(8,128)(2,1)} %refs_2_.1, bf16[128,2048]{1,0:T(8,128)(2,1)} %refs_3_.1, bf16[128,2048]{1,0:T(8,128)(2,1)} %refs_4_.1, ...), custom_call_target="tpu_custom_call" | custom-call | tf_op jit(solution)/shard_map/pallas_call | solution.py:525
  184.1 0.0 copy-done
  184.1 0.0 copy-start.2
  184.1 0.0 copy-start.1
  184.2 2.6 %convert_add_fusion = f32[256,1536]{1,0:T(8,128)} fusion(f32[256,1536]{1,0:T(8,128)S(1)} %copy-done, bf16[256,1536]{1,0:T(8,128)(2,1)} %get-tuple-element.8), kind=kLoop, calls=%fused_computation | loop fusion | flops 786432 | bytes 3932160 | tf_op jit(solution)/shard_map/add | solution.py:557
  186.7 0.0 copy-done.2
  186.7 0.8 copy.14
  187.5 0.0 copy-done.1
  187.5 0.8 copy.15
Async XLA Ops:
  0.6 183.5 %copy-start = (f32[256,1536]{1,0:T(8,128)S(1)}, f32[256,1536]{1,0:T(8,128)}, u32[]{:S(2)}) copy-start(f32[256,1536]{1,0:T(8,128)} %param.17) | copy-start | bytes 4718596
  184.1 2.6 %copy-start.2 = (bf16[2,64,2048]{2,1,0:T(8,128)(2,1)S(1)}, bf16[2,64,2048]{2,1,0:T(8,128)(2,1)}, u32[]{:S(2)}) copy-start(bf16[2,64,2048]{2,1,0:T(8,128)(2,1)} %get-tuple-element.6) | copy-start | bytes 1572868
  184.1 3.4 %copy-start.1 = (bf16[2,64,2048]{2,1,0:T(8,128)(2,1)S(1)}, bf16[2,64,2048]{2,1,0:T(8,128)(2,1)}, u32[]{:S(2)}) copy-start(bf16[2,64,2048]{2,1,0:T(8,128)(2,1)} %get-tuple-element.7) | copy-start | bytes 1572868

commit v2 on v0

--- a/solution.py
+++ b/solution.py
@@ -125,7 +125,10 @@
     def __init__(self, m, cp, p, rx, tx, rg, acc, place):
         self.m, self.cp, self.p, self.rx, self.tx, self.rg, self.acc = m, cp, p, rx, tx, rg, acc
         self.place = place
-        self.pair, self.far = {}, {}
+        self.pair, self.hops = {}, {}
+        self.side = 2 * (m.R - 1)
+        self.cross = self.side + m.R
+        self.back = self.cross + 1
 
     def start(self, t):
         m = self.m
@@ -133,33 +136,63 @@
             src = self.p.at[t, :, :, m.sibling_index(j)]
             self.pair[t, j] = self.cp.push(src, self.rx.at[j - 1, t], m.sibling(j))
 
+    def total(self, t, e, dr, dy):
+        m = self.m
+        block = lax.rem(m.r + dr, m.R) * m.fy + lax.rem(m.y + dy, m.fy)
+        value = self.p[t, e, block, m.k].astype(F32)
+        for j in range(1, m.tp):
+            value = value + self.rx[j - 1, t, e, block].astype(F32)
+        return value
+
+    def hop(self, t, first, count, dr, dy):
+        m, part = self.m, pl.ds(first, count)
+        to = m.peer(m.offsets.index((dr, dy)))
+        self.hops[t, first] = self.cp.push(self.tx.at[t, part], self.rg.at[t, part], to)
+
     def middle(self, t):
-        m, n = self.m, len(self.m.offsets)
+        m = self.m
         for j in range(1, m.tp):
             self.pair[t, j].wait_recv()
-
-        def total(block):
-            value = self.p[t, :, block, m.k].astype(F32)
-            for j in range(1, m.tp):
-                value = value + self.rx[j - 1, t, :, block].astype(F32)
-            return value
-
-        for o in range(n):
-            self.tx[t, o] = total(m.index(o)).astype(BF16)
-            self.far[t, o] = self.cp.push(self.tx.at[t, o], self.rg.at[t, o], m.peer(o))
-        self.acc[self.place(t)] = total(m.g)
+        for dr in range(1, m.R):
+            for dy in range(2):
+                self.tx[t, 2 * (dr - 1) + dy] = self.total(t, 0, dr, dy).astype(BF16)
+            self.hop(t, 2 * (dr - 1), 2, dr, 0)
+        for dr in range(m.R):
+            self.tx[t, self.side + dr] = self.total(t, 1, dr, 1).astype(BF16)
+        self.hop(t, self.side, m.R, 0, 1)
+        for e in range(2):
+            self.acc[self.place(t), e] = self.total(t, e, 0, 0)
+
+    def relay(self, t):
+        m = self.m
+
+        def got(slot):
+            return self.rg[t, slot].astype(F32)
+
+        mine, other = self.acc[self.place(t), 0], self.total(t, 0, 0, 1)
+        for dr in range(1, m.R):
+            self.hops[t, 2 * (dr - 1)].wait_recv()
+            mine, other = mine + got(2 * (dr - 1)), other + got(2 * (dr - 1) + 1)
+        self.tx[t, self.cross] = other.astype(BF16)
+        self.hop(t, self.cross, 1, 0, 1)
+        self.acc[self.place(t), 0] = mine
+        self.hops[t, self.side].wait_recv()
+        for dr in range(1, m.R):
+            value = self.total(t, 1, dr, 0) + got(self.side + dr)
+            self.tx[t, self.back + dr - 1] = value.astype(BF16)
+            self.hop(t, self.back + dr - 1, 1, dr, 0)
+        self.acc[self.place(t), 1] += got(self.side)
 
     def end(self, t):
-        n = len(self.m.offsets)
-        for o in range(n):
-            self.far[t, o].wait_recv()
-        value = self.acc[self.place(t)]
-        for o in range(n):
-            value = value + self.rg[t, o].astype(F32)
-        self.acc[self.place(t)] = value
+        m = self.m
+        self.hops[t, self.cross].wait_recv()
+        self.acc[self.place(t), 0] += self.rg[t, self.cross].astype(F32)
+        for dr in range(1, m.R):
+            self.hops[t, self.back + dr - 1].wait_recv()
+            self.acc[self.place(t), 1] += self.rg[t, self.back + dr - 1].astype(F32)
 
     def finish(self):
-        for copy in list(self.pair.values()) + list(self.far.values()):
+        for copy in list(self.pair.values()) + list(self.hops.values()):
             copy.wait_send()
 
 
@@ -314,7 +347,11 @@
         sc.start(t)
         if t:
             sc.middle(t - 1)
+        if t > 1:
+            sc.relay(t - 2)
     sc.middle(len(order) - 1)
+    sc.relay(len(order) - 2)
+    sc.relay(len(order) - 1)
     for t in range(len(order)):
         sc.end(t)
     places = [divmod(block, fy) for block in range(m.fs)]
@@ -378,7 +415,11 @@
         dsc.start(t)
         if t:
             dsc.middle(t - 1)
+        if t > 1:
+            dsc.relay(t - 2)
     dsc.middle(fz - 1)
+    dsc.relay(fz - 2)
+    dsc.relay(fz - 1)
     for s in range(2, ring_h.half + 1):
         ring_h.step(s)
     dz[m.z] = jnp.stack([dall[:, t, pl.ds(m.z * fy, fy)] for t in range(tp)])
@@ -387,6 +428,20 @@
         src = m.along(-s)
         for j in range(1, tp):
             passed.append(cp.push(dz.at[src, m.k], dz.at[src, m.k], m.sibling(j)))
+    for copy in passed:
+        copy.wait()
+    sends = []
+
+    def gradient(r, e):
+        a = dz[:, :, pl.ds(r * fy, fy), e]
+        b = hout[:, :, pl.ds(r * fy, fy)]
+        return dot(flat(a), flat(b), 0, 0).astype(BF16)
+
+    for o in range(n):
+        r, y = m.moved(o)
+        dw[o] = gradient(r, y)
+        sends.append(cp.push(dw.at[o], owned_at(m.g), m.peer(o)))
+    owned_at(m.g)[...] = gradient(m.r, m.y)
     for t in range(fz):
         dsc.end(t)
     xf = x_early[mine].astype(F32)
@@ -399,20 +454,6 @@
         v = rs * (gained(t, e) - xf[:, cols] * factor)
         dx_out[m.k, :, cols] = (cot[mine, cols].astype(F32) + v).astype(BF16)
     last = [cp.push(dx_out.at[m.k], dx_out.at[m.k], m.sibling(j)) for j in range(1, tp)]
-    for copy in passed:
-        copy.wait()
-    sends = []
-
-    def gradient(r, e):
-        a = dz[:, :, pl.ds(r * fy, fy), e]
-        b = hout[:, :, pl.ds(r * fy, fy)]
-        return dot(flat(a), flat(b), 0, 0).astype(BF16)
-
-    for o in range(n):
-        r, y = m.moved(o)
-        dw[o] = gradient(r, y)
-        sends.append(cp.push(dw.at[o], owned_at(m.g), m.peer(o)))
-    owned_at(m.g)[...] = gradient(m.r, m.y)
     for copy in sends + last + late:
         copy.wait()
     for copies in (xs, ys, dg, across):
@@ -441,14 +482,14 @@
         weights = [jnp.stack([w.reshape(drows, G, part) for w in weights]).transpose(2, 0, 1, 3)]
     ring = 2 * (fz // 2)
     count = (3 * (fy - 1) + ring * (3 * fy + tp) + 2 * (n + n * (tp - 1)) + 3 * (tp - 1)
-             + 2 * fz * (tp - 1 + n) + (fz - 1) * tp + n)
+             + 2 * fz * (tp - 1 + 2 * R) + (fz - 1) * tp + n)
 
     def scatter(c):
         return [
             V((fz, fy, G, tp, c, drows), BF16),
             V((tp - 1, fz, fy, G, c, drows), BF16),
-            V((fz, n, fy, c, drows), BF16),
-            V((fz, n, fy, c, drows), BF16),
+            V((fz, 4 * R - 2, c, drows), BF16),
+            V((fz, 4 * R - 2, c, drows), BF16),
             V((fz, fy, c, drows), F32),
         ]
 

time: 157 us -> 155 us (0.987)
  no operation moved by 1% of the time
where the time goes in v2:
time: 155 us; the launch traced here: 153 us
  Pallas kernels  148 us (95%)
  other arithmetic  2.55 us (2%)
  local copies, waits for them, and re-layouts  1.6 us (1%)
    pallas_call x1, Pallas kernels, body(): pl.pallas_call(functools.partial(kernel, sizes, D, len(weights)), out_sha...  148 us

profile of v2, /device:TPU:0, one launch (start us, length us, event | category | flops | bytes accessed | tf_op | source)
XLA Modules:
  0.0 153.0 jit_solution(2954903134052062053)
XLA Ops:
  0.6 0.0 copy-start
  0.6 148.2 %shard_map.112 = (bf16[2,64,2048]{2,1,0:T(8,128)(2,1)}, bf16[2,64,2048]{2,1,0:T(8,128)(2,1)}, bf16[256,1536]{1,0:T(8,128)(2,1)}) custom-call(bf16[256,1536]{1,0:T(8,128)(2,1)} %refs_0_.1, bf16[256,1536]{1,0:T(8,128)(2,1)} %refs_1_.1, bf16[256,1536]{1,0:T(8,128)(2,1)} %refs_2_.1, bf16[128,2048]{1,0:T(8,128)(2,1)} %refs_3_.1, bf16[128,2048]{1,0:T(8,128)(2,1)} %refs_4_.1, ...), custom_call_target="tpu_custom_call" | custom-call | tf_op jit(solution)/shard_map/pallas_call | solution.py:497
  148.9 0.0 copy-done
  148.9 0.0 copy-start.2
  148.9 0.0 copy-start.1
  148.9 2.6 %convert_add_fusion = f32[256,1536]{1,0:T(8,128)} fusion(f32[256,1536]{1,0:T(8,128)S(1)} %copy-done, bf16[256,1536]{1,0:T(8,128)(2,1)} %get-tuple-element.8), kind=kLoop, calls=%fused_computation | loop fusion | flops 786432 | bytes 3932160 | tf_op jit(solution)/shard_map/add | solution.py:529
  151.4 0.0 copy-done.2
  151.4 0.8 copy.14
  152.2 0.0 copy-done.1
  152.2 0.8 copy.15
Async XLA Ops:
  0.6 148.2 %copy-start = (f32[256,1536]{1,0:T(8,128)S(1)}, f32[256,1536]{1,0:T(8,128)}, u32[]{:S(2)}) copy-start(f32[256,1536]{1,0:T(8,128)} %param.17) | copy-start | bytes 4718596
  148.9 2.6 %copy-start.2 = (bf16[2,64,2048]{2,1,0:T(8,128)(2,1)S(1)}, bf16[2,64,2048]{2,1,0:T(8,128)(2,1)}, u32[]{:S(2)}) copy-start(bf16[2,64,2048]{2,1,0:T(8,128)(2,1)} %get-tuple-element.6) | copy-start | bytes 1572868
  148.9 3.4 %copy-start.1 = (bf16[2,64,2048]{2,1,0:T(8,128)(2,1)S(1)}, bf16[2,64,2048]{2,1,0:T(8,128)(2,1)}, u32[]{:S(2)}) copy-start(bf16[2,64,2048]{2,1,0:T(8,128)(2,1)} %get-tuple-element.7) | copy-start | bytes 1572868

commit v3 on v2

--- a/solution.py
+++ b/solution.py
@@ -122,9 +122,9 @@
 
 
 class Scatter:
-    def __init__(self, m, cp, p, rx, tx, rg, acc, place):
+    def __init__(self, m, cp, p, rx, tx, rg, acc, place, its=slice(None)):
         self.m, self.cp, self.p, self.rx, self.tx, self.rg, self.acc = m, cp, p, rx, tx, rg, acc
-        self.place = place
+        self.place, self.its = place, its
         self.pair, self.hops = {}, {}
         self.side = 2 * (m.R - 1)
         self.cross = self.side + m.R
@@ -133,21 +133,21 @@
     def start(self, t):
         m = self.m
         for j in range(1, m.tp):
-            src = self.p.at[t, :, :, m.sibling_index(j)]
-            self.pair[t, j] = self.cp.push(src, self.rx.at[j - 1, t], m.sibling(j))
+            src = self.p.at[t, :, :, m.sibling_index(j), self.its]
+            self.pair[t, j] = self.cp.push(src, self.rx.at[j - 1, t, :, :, self.its], m.sibling(j))
 
     def total(self, t, e, dr, dy):
         m = self.m
         block = lax.rem(m.r + dr, m.R) * m.fy + lax.rem(m.y + dy, m.fy)
-        value = self.p[t, e, block, m.k].astype(F32)
+        value = self.p[t, e, block, m.k, self.its].astype(F32)
         for j in range(1, m.tp):
-            value = value + self.rx[j - 1, t, e, block].astype(F32)
+            value = value + self.rx[j - 1, t, e, block, self.its].astype(F32)
         return value
 
     def hop(self, t, first, count, dr, dy):
         m, part = self.m, pl.ds(first, count)
         to = m.peer(m.offsets.index((dr, dy)))
-        self.hops[t, first] = self.cp.push(self.tx.at[t, part], self.rg.at[t, part], to)
+        self.hops[t, first] = self.cp.push(self.tx.at[t, part, self.its], self.rg.at[t, part, self.its], to)
 
     def middle(self, t):
         m = self.m
@@ -155,41 +155,41 @@
             self.pair[t, j].wait_recv()
         for dr in range(1, m.R):
             for dy in range(2):
-                self.tx[t, 2 * (dr - 1) + dy] = self.total(t, 0, dr, dy).astype(BF16)
+                self.tx[t, 2 * (dr - 1) + dy, self.its] = self.total(t, 0, dr, dy).astype(BF16)
             self.hop(t, 2 * (dr - 1), 2, dr, 0)
         for dr in range(m.R):
-            self.tx[t, self.side + dr] = self.total(t, 1, dr, 1).astype(BF16)
+            self.tx[t, self.side + dr, self.its] = self.total(t, 1, dr, 1).astype(BF16)
         self.hop(t, self.side, m.R, 0, 1)
         for e in range(2):
-            self.acc[self.place(t), e] = self.total(t, e, 0, 0)
+            self.acc[self.place(t), e, self.its] = self.total(t, e, 0, 0)
 
     def relay(self, t):
         m = self.m
 
         def got(slot):
-            return self.rg[t, slot].astype(F32)
-
-        mine, other = self.acc[self.place(t), 0], self.total(t, 0, 0, 1)
+            return self.rg[t, slot, self.its].astype(F32)
+
+        mine, other = self.acc[self.place(t), 0, self.its], self.total(t, 0, 0, 1)
         for dr in range(1, m.R):
             self.hops[t, 2 * (dr - 1)].wait_recv()
             mine, other = mine + got(2 * (dr - 1)), other + got(2 * (dr - 1) + 1)
-        self.tx[t, self.cross] = other.astype(BF16)
+        self.tx[t, self.cross, self.its] = other.astype(BF16)
         self.hop(t, self.cross, 1, 0, 1)
-        self.acc[self.place(t), 0] = mine
+        self.acc[self.place(t), 0, self.its] = mine
         self.hops[t, self.side].wait_recv()
         for dr in range(1, m.R):
             value = self.total(t, 1, dr, 0) + got(self.side + dr)
-            self.tx[t, self.back + dr - 1] = value.astype(BF16)
+            self.tx[t, self.back + dr - 1, self.its] = value.astype(BF16)
             self.hop(t, self.back + dr - 1, 1, dr, 0)
-        self.acc[self.place(t), 1] += got(self.side)
+        self.acc[self.place(t), 1, self.its] += got(self.side)
 
     def end(self, t):
         m = self.m
         self.hops[t, self.cross].wait_recv()
-        self.acc[self.place(t), 0] += self.rg[t, self.cross].astype(F32)
+        self.acc[self.place(t), 0, self.its] += self.rg[t, self.cross, self.its].astype(F32)
         for dr in range(1, m.R):
             self.hops[t, self.back + dr - 1].wait_recv()
-            self.acc[self.place(t), 1] += self.rg[t, self.back + dr - 1].astype(F32)
+            self.acc[self.place(t), 1, self.its] += self.rg[t, self.back + dr - 1, self.its].astype(F32)
 
     def finish(self):
         for copy in list(self.pair.values()) + list(self.hops.values()):
@@ -209,7 +209,11 @@
 
 
 def kernel(sizes, D, nw, *refs):
-    ws, refs = refs[:nw], refs[nw:]
+    away, refs = refs[:nw], refs[nw:]
+    ws, load, refs = refs[-nw - 1:-1], refs[-1], refs[:-nw - 1]
+    loads = [pltpu.make_async_copy(away[i], ws[i], load.at[i]) for i in range(nw)]
+    for copy in loads:
+        copy.start()
     (x_late, x_early, cot, pre_gain, post_gain, y_out, dx_out, owned_out,
      wout, xout, dpost, gate, up, hid, hout, p, rx, tx, rg, acc, dall, dhid, dgate, dup, dz,
            q, qx, qt, qg, dacc, dw, sems) = refs
@@ -217,6 +221,8 @@
     cp = Copies(sems)
     n, fy, tp, fz = len(m.offsets), m.fy, m.tp, m.fz
     m.barrier(group=True, pair=True, levels=True)
+    for copy in loads:
+        copy.wait()
     f = m.z * fy + m.y
     rows, part = x_late.shape[0], wout.shape[-1]
     ce, drows = rows // tp, D // m.fs
@@ -327,7 +333,8 @@
     ring_h = Ring(m, cp, lambda c: hout.at[m.z, c], lambda z, c: hout.at[z, c], list(range(tp)))
 
     order = stages(m)
-    sc = Scatter(m, cp, p, rx, tx, rg, acc, lambda t: m.along(order[t][0]))
+    halves = [pl.ds(low, ce) for low in (ce, 0)]
+    sc, sl = (Scatter(m, cp, p, rx, tx, rg, acc, lambda t: m.along(order[t][0]), its) for its in halves)
     for t, (dist, s, ds) in enumerate(order):
         for d in ds:
             ring_b.step(s, (d,))
@@ -345,6 +352,7 @@
 
             lax.fori_loop(0, m.G, product, 0)
         sc.start(t)
+        sl.start(t)
         if t:
             sc.middle(t - 1)
         if t > 1:
@@ -367,13 +375,9 @@
     dg = {o: cp.push(dall.at[m.g, m.k], dall.at[m.g, m.k], m.peer(o)) for o in range(n)}
     own = [cp.push(dall.at[m.g, m.k], dall.at[m.g, m.k], m.sibling(j)) for j in range(1, tp)]
     ring_h.step(1)
-    late_rz = lax.rsqrt(row_sum(lambda t, e: acc[t, e, :ce] * acc[t, e, :ce]) / D + eps)
-    for t, e in places:
-        cols = columns(t * fy + e)
-        v = 0.5 * acc[t, e, :ce] * late_rz * post_gain[:, cols]
-        y_out[m.k, :, cols] = (x_late[mine, cols].astype(F32) + v).astype(BF16)
+    for t in range(len(order)):
+        sl.middle(t)
     spread(dg, dall)
-    late = [cp.push(y_out.at[m.k], y_out.at[m.k], m.sibling(j)) for j in range(1, tp)]
     across = {}
     for s in range(1, fz):
         src = dall.at[:, m.k, pl.ds(m.along(s) * fy, fy)]
@@ -401,6 +405,8 @@
         return carry
 
     lax.fori_loop(0, m.G, gates, 0)
+    for t in range(len(order)):
+        sl.relay(t)
     dsc = Scatter(m, cp, q, qx, qt, qg, dacc, lambda t: t)
     for t in range(fz):
         for e in range(fy):
@@ -437,11 +443,19 @@
         b = hout[:, :, pl.ds(r * fy, fy)]
         return dot(flat(a), flat(b), 0, 0).astype(BF16)
 
-    for o in range(n):
+    for o in reversed(range(n)):
         r, y = m.moved(o)
         dw[o] = gradient(r, y)
         sends.append(cp.push(dw.at[o], owned_at(m.g), m.peer(o)))
     owned_at(m.g)[...] = gradient(m.r, m.y)
+    for t in range(len(order)):
+        sl.end(t)
+    late_rz = lax.rsqrt(row_sum(lambda t, e: acc[t, e, :ce] * acc[t, e, :ce]) / D + eps)
+    for t, e in places:
+        cols = columns(t * fy + e)
+        v = 0.5 * acc[t, e, :ce] * late_rz * post_gain[:, cols]
+        y_out[m.k, :, cols] = (x_late[mine, cols].astype(F32) + v).astype(BF16)
+    late = [cp.push(y_out.at[m.k], y_out.at[m.k], m.sibling(j)) for j in range(1, tp)]
     for t in range(fz):
         dsc.end(t)
     xf = x_early[mine].astype(F32)
@@ -459,7 +473,7 @@
     for copies in (xs, ys, dg, across):
         for copy in copies.values():
             copy.wait_send()
-    for thing in (ring_a, ring_b, ring_h, sc, dsc):
+    for thing in (ring_a, ring_b, ring_h, sc, sl, dsc):
         thing.finish()
 
 
@@ -482,7 +496,7 @@
         weights = [jnp.stack([w.reshape(drows, G, part) for w in weights]).transpose(2, 0, 1, 3)]
     ring = 2 * (fz // 2)
     count = (3 * (fy - 1) + ring * (3 * fy + tp) + 2 * (n + n * (tp - 1)) + 3 * (tp - 1)
-             + 2 * fz * (tp - 1 + 2 * R) + (fz - 1) * tp + n)
+             + 3 * fz * (tp - 1 + 2 * R) + (fz - 1) * tp + n)
 
     def scatter(c):
         return [
@@ -500,7 +514,7 @@
             S((tp, ce, D), BF16), S((tp, ce, D), BF16),
             S((drows, width) if aligned else (G, drows, part), BF16),
         ],
-        in_specs=[VMEM] * (len(weights) + 5),
+        in_specs=[pl.BlockSpec(memory_space=pl.ANY)] * len(weights) + [VMEM] * 5,
         out_specs=[VMEM] * 3,
         scratch_shapes=[
             V((3, fs, drows, part), BF16),
@@ -519,7 +533,7 @@
         ] + scatter(ce) + [
             V((n, drows, part), BF16),
             DMA((2, count)),
-        ],
+        ] + [V(w.shape, w.dtype) for w in weights] + [DMA((len(weights),))],
         compiler_params=pltpu.CompilerParams(
             collective_id=0, has_side_effects=True, vmem_limit_bytes=60 * 1024 * 1024
         ),

time: 155 us -> 154 us (level)
  no operation moved by 1% of the time
where the time goes in v3:
time: 154 us; the launch traced here: 152 us
  Pallas kernels  147 us (95%)
  other arithmetic  2.55 us (2%)
  local copies, waits for them, and re-layouts  1.6 us (1%)
    pallas_call x1, Pallas kernels, body(): pl.pallas_call(functools.partial(kernel, sizes, D, len(weights)), out_sha...  147 us

profile of v3, /device:TPU:0, one launch (start us, length us, event | category | flops | bytes accessed | tf_op | source)
XLA Modules:
  0.0 151.6 jit_solution(17102925176479932225)
XLA Ops:
  0.6 0.0 copy-start
  0.6 146.8 %shard_map.112 = (bf16[2,64,2048]{2,1,0:T(8,128)(2,1)}, bf16[2,64,2048]{2,1,0:T(8,128)(2,1)}, bf16[256,1536]{1,0:T(8,128)(2,1)}) custom-call(bf16[256,1536]{1,0:T(8,128)(2,1)} %refs_0_.1, bf16[256,1536]{1,0:T(8,128)(2,1)} %refs_1_.1, bf16[256,1536]{1,0:T(8,128)(2,1)} %refs_2_.1, bf16[128,2048]{1,0:T(8,128)(2,1)} %refs_3_.1, bf16[128,2048]{1,0:T(8,128)(2,1)} %refs_4_.1, ...), custom_call_target="tpu_custom_call" | custom-call | tf_op jit(solution)/shard_map/pallas_call | solution.py:511
  147.4 0.0 copy-done
  147.5 0.0 copy-start.2
  147.5 0.0 copy-start.1
  147.5 2.6 %convert_add_fusion = f32[256,1536]{1,0:T(8,128)} fusion(f32[256,1536]{1,0:T(8,128)S(1)} %copy-done, bf16[256,1536]{1,0:T(8,128)(2,1)} %get-tuple-element.8), kind=kLoop, calls=%fused_computation | loop fusion | flops 786432 | bytes 3932160 | tf_op jit(solution)/shard_map/add | solution.py:543
  150.0 0.0 copy-done.2
  150.0 0.8 copy.14
  150.8 0.0 copy-done.1
  150.8 0.8 copy.15
Async XLA Ops:
  0.6 146.8 %copy-start = (f32[256,1536]{1,0:T(8,128)S(1)}, f32[256,1536]{1,0:T(8,128)}, u32[]{:S(2)}) copy-start(f32[256,1536]{1,0:T(8,128)} %param.17) | copy-start | bytes 4718596
  147.5 2.6 %copy-start.2 = (bf16[2,64,2048]{2,1,0:T(8,128)(2,1)S(1)}, bf16[2,64,2048]{2,1,0:T(8,128)(2,1)}, u32[]{:S(2)}) copy-start(bf16[2,64,2048]{2,1,0:T(8,128)(2,1)} %get-tuple-element.6) | copy-start | bytes 1572868
  147.5 3.4 %copy-start.1 = (bf16[2,64,2048]{2,1,0:T(8,128)(2,1)S(1)}, bf16[2,64,2048]{2,1,0:T(8,128)(2,1)}, u32[]{:S(2)}) copy-start(bf16[2,64,2048]{2,1,0:T(8,128)(2,1)} %get-tuple-element.7) | copy-start | bytes 1572868

commit v4 on v3

--- a/solution.py
+++ b/solution.py
@@ -296,11 +296,8 @@
 
     spread(xs, xout)
     ring_a.step(1)
-    for e in range(fy):
-        if e:
-            ys[(fy - e) % fy, 2].wait_recv()
-        for d in (0, 1):
-            ring_b.send(d, 1, (e, 2))
+    for d in (0, 1):
+        ring_b.send(d, 1, (0, 2))
     for copy in passed:
         copy.wait()
     passed.clear()
@@ -310,6 +307,11 @@
     for dist, s, ds in stages(m):
         for d in ds:
             ring_a.step(s, (d,))
+        if s == m.fz // 2:
+            for e in range(1, fy):
+                ys[(fy - e) % fy, 2].wait_recv()
+                for d in (0, 1):
+                    ring_b.send(d, 1, (e, 2))
         zt = m.along(dist)
         for e in range(fy):
             block = zt * fy + e

time: 154 us -> 154 us (level)
  no operation moved by 1% of the time
where the time goes in v4:
time: 154 us; the launch traced here: 152 us
  Pallas kernels  147 us (95%)
  other arithmetic  2.55 us (2%)
  local copies, waits for them, and re-layouts  1.6 us (1%)
    pallas_call x1, Pallas kernels, body(): pl.pallas_call(functools.partial(kernel, sizes, D, len(weights)), out_sha...  147 us

profile of v4, /device:TPU:0, one launch (start us, length us, event | category | flops | bytes accessed | tf_op | source)
XLA Modules:
  0.0 151.6 jit_solution(15793627928935923293)
XLA Ops:
  0.6 0.0 copy-start
  0.6 146.8 %shard_map.112 = (bf16[2,64,2048]{2,1,0:T(8,128)(2,1)}, bf16[2,64,2048]{2,1,0:T(8,128)(2,1)}, bf16[256,1536]{1,0:T(8,128)(2,1)}) custom-call(bf16[256,1536]{1,0:T(8,128)(2,1)} %refs_0_.1, bf16[256,1536]{1,0:T(8,128)(2,1)} %refs_1_.1, bf16[256,1536]{1,0:T(8,128)(2,1)} %refs_2_.1, bf16[128,2048]{1,0:T(8,128)(2,1)} %refs_3_.1, bf16[128,2048]{1,0:T(8,128)(2,1)} %refs_4_.1, ...), custom_call_target="tpu_custom_call" | custom-call | tf_op jit(solution)/shard_map/pallas_call | solution.py:513
  147.4 0.0 copy-done
  147.5 0.0 copy-start.2
  147.5 0.0 copy-start.1
  147.5 2.6 %convert_add_fusion = f32[256,1536]{1,0:T(8,128)} fusion(f32[256,1536]{1,0:T(8,128)S(1)} %copy-done, bf16[256,1536]{1,0:T(8,128)(2,1)} %get-tuple-element.8), kind=kLoop, calls=%fused_computation | loop fusion | flops 786432 | bytes 3932160 | tf_op jit(solution)/shard_map/add | solution.py:545
  150.0 0.0 copy-done.2
  150.0 0.8 copy.14
  150.8 0.0 copy-done.1
  150.8 0.8 copy.15
Async XLA Ops:
  0.6 146.8 %copy-start = (f32[256,1536]{1,0:T(8,128)S(1)}, f32[256,1536]{1,0:T(8,128)}, u32[]{:S(2)}) copy-start(f32[256,1536]{1,0:T(8,128)} %param.17) | copy-start | bytes 4718596
  147.5 2.6 %copy-start.2 = (bf16[2,64,2048]{2,1,0:T(8,128)(2,1)S(1)}, bf16[2,64,2048]{2,1,0:T(8,128)(2,1)}, u32[]{:S(2)}) copy-start(bf16[2,64,2048]{2,1,0:T(8,128)(2,1)} %get-tuple-element.6) | copy-start | bytes 1572868
  147.5 3.4 %copy-start.1 = (bf16[2,64,2048]{2,1,0:T(8,128)(2,1)S(1)}, bf16[2,64,2048]{2,1,0:T(8,128)(2,1)}, u32[]{:S(2)}) copy-start(bf16[2,64,2048]{2,1,0:T(8,128)(2,1)} %get-tuple-element.7) | copy-start | bytes 1572868
